TPU v7x, 32 devices: a whole 2x2x4 slice. The times are simulated.
32 devices in a mesh: sp: 4 (over y, x), tp: 8 (over z, core).
Axes of the slice: x: 2, y: 2, z: 4, core: 2. Of those that a mesh axis runs over, the one named last changes fastest.
Arguments:
- queries: bfloat16 [1536, 2048], P('sp', 'tp'), may hold values from -6 to 6
- cell_key_rows: bfloat16 [1536, 2048], P('sp', 'tp'), may hold values from -6 to 6
- cell_value_rows: bfloat16 [1536, 2048], P('sp', 'tp'), may hold values from -6 to 6
- output_gate_logits: bfloat16 [1536, 2048], P('sp', 'tp'), may hold values from -6 to 6
- input_gate_logs: float32 [16, 1536], P('tp', 'sp'), may hold values from -5 to 250
- forget_gate_logits: float32 [16, 1536], P('tp', 'sp'), may hold values from 1 to 13
- extra_log_forget: float32 [16, 1536], P('tp', 'sp'), may hold values from -0.7 to 0
- head_norm_gain: float32 [2048], P('tp'), may hold values from 0.1 to 1.9
- cell_output_matrix: bfloat16 [2048, 4096], P('tp'), may hold values from -0.125 to 0.125
- residual: bfloat16 [1536, 4096], P('sp'), may hold values from -6 to 6
- expert_norm_gain: float32 [4096], replicated, may hold values from 0.1 to 1.9
- routes: int32 [1536, 2], P('sp'), may hold values from 0 to 3, all different within a row; in each aligned block of 48 rows (0 to 47, 48 to 95, ...) at most 48 rows name the same one
- token_expert_weights: float32 [1536, 2], P('sp'), may hold values from 0.2 to 1
- expert_gate_matrix: bfloat16 [4, 4096, 2048], P('sp', None, 'tp'), may hold values from -0.09375 to 0.09375
- expert_up_matrix: bfloat16 [4, 4096, 2048], P('sp', None, 'tp'), may hold values from -0.09375 to 0.09375
- expert_down_matrix: bfloat16 [4, 2048, 4096], P('sp', 'tp'), may hold values from -0.125 to 0.125
Outputs:
- layer_out: bfloat16 [1536, 4096], P(('sp', 'tp'))
Inputs may be any that keep to these rules, and one draw needn't show every extreme that they name: `routes`: each row names 2 different experts. In the rows of one device (aligned blocks of 48 rows) no expert is named more than 48 times, and in some blocks one expert is named exactly 48 times.
All inputs are finite; a program needn't handle non-finite values.
Results may differ from a plain program's by a relative error of at most 0.019.
Values may be sent and summed in bfloat16 or wider, within the bound.
A program may use at most 128 MiB of HBM per device.

v0:
```python
import jax
import jax.numpy as jnp
from jax import lax
from jax.sharding import PartitionSpec as P

HEAD_DIM = 128
BLOCK = 128
floor_neg = -1e30
norm_eps = 1e-06


def entering(x, axis, combine, identity):
    count, here = (lax.axis_size(axis), lax.axis_index(axis))
    everything = jax.tree.map(lambda part: lax.all_gather(part, axis), x)
    start = jax.tree.map(
        lambda part, zero: jnp.broadcast_to(jnp.asarray(zero, part.dtype), part.shape), x, identity
    )

    def lap(k, before):
        reached = k < here
        new = combine(before, jax.tree.map(lambda part: part[k], everything))
        return jax.tree.map(lambda a, b: jnp.where(reached, a, b), new, before)

    return lax.fori_loop(0, count, lap, start)


def block_cells(query_f, key_f, value_f, input_f, forget_log_values, start_cell, start_stab):
    heads, length, width = query_f.shape
    count = length // BLOCK
    highest = lax.Precision.HIGHEST

    def split(array):
        return jnp.moveaxis(array.reshape((heads, count, BLOCK) + array.shape[2:]), 1, 0)

    causal = jnp.tril(jnp.ones((BLOCK, BLOCK), dtype=bool))

    def advance(carry, block):
        cell, stab = carry
        qblock, kblock, vblock, iblock, fblock = block
        cumul = jnp.cumsum(fblock, axis=-1)
        total = cumul[:, -1]
        log_inner = jnp.where(
            causal[None], cumul[:, :, None] - cumul[:, None, :] + iblock[:, None, :], floor_neg
        )
        carried = cumul + stab[:, None]
        stab_row = jnp.maximum(carried, jnp.max(log_inner, axis=-1))
        scores = jnp.einsum("hld,hsd->hls", qblock, kblock, precision=highest) * jnp.exp(
            log_inner - stab_row[..., None]
        )
        numer = jnp.einsum("hls,hsd->hld", scores, vblock, precision=highest) + jnp.exp(
            carried - stab_row
        )[..., None] * jnp.einsum("hld,hde->hle", qblock, cell, precision=highest)
        log_write = total[:, None] - cumul + iblock
        stab_next = jnp.maximum(total + stab, jnp.max(log_write, axis=-1))
        weights = jnp.exp(log_write - stab_next[:, None])
        cell_next = jnp.exp(total + stab - stab_next)[:, None, None] * cell + jnp.einsum(
            "hsd,hse->hde", kblock * weights[..., None], vblock, precision=highest
        )
        return ((cell_next, stab_next), (numer, stab_row))

    inputs = tuple(
        (split(array) for array in (query_f, key_f, value_f, input_f, forget_log_values))
    )
    unused, (numer, stab_rows) = lax.scan(advance, (start_cell, start_stab), inputs)
    numer = jnp.moveaxis(numer, 0, 1).reshape(heads, length, width)
    stab_rows = jnp.moveaxis(stab_rows, 0, 1).reshape(heads, length)
    return (numer, stab_rows)


def combine_states(earlier, later):
    cell_early, stab_early, total_early = earlier
    cell_late, stab_late, total_late = later
    stab = jnp.maximum(total_late + stab_early, stab_late)
    cell = (
        jnp.exp(total_late + stab_early - stab)[:, None, None] * cell_early
        + jnp.exp(stab_late - stab)[:, None, None] * cell_late
    )
    return (cell, stab, total_early + total_late)


def rms_scale(rows, gain):
    values = rows.astype(jnp.float32)
    return (
        values * lax.rsqrt(jnp.mean(values * values, axis=-1, keepdims=True) + norm_eps) * gain
    ).astype(jnp.bfloat16)


def slot_tables(block_routes, experts, capacity):
    flat = block_routes.reshape(-1)
    count = flat.shape[0]
    topk = block_routes.shape[1]
    onehot = (flat[:, None] == jnp.arange(experts, dtype=jnp.int32)[None, :]).astype(jnp.int32)
    before = jnp.cumsum(onehot, axis=0) - onehot
    position = jnp.sum(before * onehot, axis=1)
    slot = flat * capacity + position
    match = slot[None, :] == jnp.arange(experts * capacity, dtype=jnp.int32)[:, None]
    owner = jnp.arange(count, dtype=jnp.int32)[None, :] // topk + 1
    source = jnp.sum(jnp.where(match, owner, 0), axis=1) - 1
    return (slot, source)


def fill_slots(rows, source):
    picked = rows[jnp.maximum(source, 0)]
    return jnp.where((source >= 0)[:, None], picked, jnp.zeros_like(picked))


def local(
    queries,
    cell_key_rows,
    cell_value_rows,
    output_gate_logits,
    input_gate_logs,
    forget_gate_logits,
    extra_log_forget,
    head_norm_gain,
    cell_output_matrix,
    residual,
    expert_norm_gain,
    routes,
    token_expert_weights,
    expert_gate_matrix,
    expert_up_matrix,
    expert_down_matrix,
):
    length = queries.shape[0]
    heads = queries.shape[1] // HEAD_DIM
    tp_count = lax.axis_size("tp")
    experts = lax.axis_size("sp")
    topk = routes.shape[1]
    tokens = length // tp_count
    capacity = max(2, 2 * tokens * topk // experts)
    highest = lax.Precision.HIGHEST
    tp_index = lax.axis_index("tp")

    def heads_of(array):
        return jnp.transpose(array.astype(jnp.float32).reshape(length, heads, HEAD_DIM), (1, 0, 2))

    query_f = heads_of(queries)
    key_f = heads_of(cell_key_rows) * HEAD_DIM ** (-0.5)
    value_f = heads_of(cell_value_rows)
    forget_log_values = jax.nn.log_sigmoid(forget_gate_logits) + extra_log_forget
    running = jnp.cumsum(forget_log_values, axis=1)
    total_dev = running[:, -1]
    log_write = input_gate_logs + total_dev[:, None] - running
    stab_dev = jnp.max(log_write, axis=1)
    cell_dev = jnp.einsum(
        "hsd,hse->hde",
        key_f * jnp.exp(log_write - stab_dev[:, None])[..., None],
        value_f,
        precision=highest,
    )
    identity = (
        jnp.zeros_like(cell_dev),
        jnp.full_like(stab_dev, floor_neg),
        jnp.zeros_like(total_dev),
    )
    prefix_cell, prefix_stab, prefix_total = entering(
        (cell_dev, stab_dev, total_dev), "sp", combine_states, identity
    )
    start_stab = jnp.maximum(prefix_stab, prefix_total)
    start_cell = jnp.exp(prefix_stab - start_stab)[:, None, None] * prefix_cell
    numer = block_cells(
        query_f, key_f, value_f, input_gate_logs, forget_log_values, start_cell, start_stab
    )[0]
    scaled = (
        numer
        * lax.rsqrt(jnp.mean(numer * numer, axis=2, keepdims=True) + norm_eps)
        * head_norm_gain.reshape(heads, 1, HEAD_DIM)
    )
    mixed = jnp.transpose(scaled, (1, 0, 2)).reshape(length, heads * HEAD_DIM)
    cell_out = (jax.nn.sigmoid(output_gate_logits.astype(jnp.float32)) * mixed).astype(jnp.bfloat16)
    gate_local = expert_gate_matrix[0]
    up_local = expert_up_matrix[0]
    down_local = expert_down_matrix[0]
    projected = lax.psum_scatter(
        jnp.dot(cell_out, cell_output_matrix, preferred_element_type=jnp.float32).astype(
            jnp.bfloat16
        ),
        "tp",
        scatter_dimension=0,
        tiled=True,
    ).astype(jnp.float32)
    own_residual = lax.dynamic_slice_in_dim(residual, tp_index * tokens, tokens, 0)
    after_mix = (own_residual.astype(jnp.float32) + projected).astype(jnp.bfloat16)
    own_routes = lax.dynamic_slice_in_dim(routes, tp_index * tokens, tokens, 0)
    slot, source = slot_tables(own_routes, experts, capacity)
    moe_in = rms_scale(after_mix, expert_norm_gain)
    sent = fill_slots(moe_in, source).reshape(experts, capacity, moe_in.shape[1])
    arrived = lax.all_to_all(sent, "sp", split_axis=0, concat_axis=0, tiled=True)
    piece = lax.all_gather(arrived, "tp", axis=0, tiled=True)
    gate = jnp.einsum("rcd,df->rcf", piece, gate_local, preferred_element_type=jnp.float32)
    upper = jnp.einsum("rcd,df->rcf", piece, up_local, preferred_element_type=jnp.float32)
    hidden = (jax.nn.silu(gate) * upper).astype(jnp.bfloat16)
    summed = lax.psum_scatter(
        jnp.einsum("rcf,fd->rcd", hidden, down_local, preferred_element_type=jnp.float32).astype(
            jnp.bfloat16
        ),
        "tp",
        scatter_dimension=0,
        tiled=True,
    )
    returned = lax.all_to_all(summed, "sp", split_axis=0, concat_axis=0, tiled=True)
    width = returned.shape[2]
    chosen = returned.reshape(experts * capacity, width)[slot].reshape(tokens, topk, width)
    own_weight = lax.dynamic_slice_in_dim(token_expert_weights, tp_index * tokens, tokens, 0)
    moe = jnp.sum(own_weight[:, :, None] * chosen.astype(jnp.float32), axis=1)
    return (after_mix.astype(jnp.float32) + moe).astype(jnp.bfloat16)


def solution(mesh):
    placed = (
        P("sp", "tp"),
        P("sp", "tp"),
        P("sp", "tp"),
        P("sp", "tp"),
        P("tp", "sp"),
        P("tp", "sp"),
        P("tp", "sp"),
        P("tp"),
        P("tp", None),
        P("sp", None),
        P(),
        P("sp", None),
        P("sp", None),
        P("sp", None, "tp"),
        P("sp", None, "tp"),
        P("sp", "tp", None),
    )
    return jax.shard_map(
        local, mesh=mesh, in_specs=placed, out_specs=P(("sp", "tp"), None), check_vma=False
    )
```

profile of v0, /device:TPU:0, one launch (start us, length us, event | category | flops | bytes accessed | tf_op | source)
XLA Modules:
  0.0 442.5 jit_solution(5801461110125140041)
XLA Ops:
  6.5 0.9 fusion.70
  7.4 0.7 fusion.69
  8.2 0.6 reduce-window.6
  9.4 0.9 fusion.61
  10.3 1.3 dynamic-slice
  12.7 11.4 %all-reduce.2 = (f32[8]{0:T(128)S(1)}, f32[8]{0:T(128)S(1)}) all-reduce(f32[8]{0:T(128)S(1)} %dynamic-update-slice, f32[8]{0:T(128)S(1)} %dynamic-update-slice.1), channel_id=2, replica_groups=mesh['sp'=4,'tp'=8] {'sp'}, use_global_device_ids=true, to_apply=%add | all-reduce | flops 16 | bytes 128
  24.1 0.7 reshape.312
  24.9 1.1 copy.71
  26.0 1.1 copy.72
  27.7 9.8 %all-gather.2 = f32[8,128,128]{2,1,0:T(8,128)S(1)} all-gather(f32[2,128,128]{2,1,0:T(8,128)S(1)} %fusion.49), channel_id=4, replica_groups=mesh['sp'=4,'tp'=8] {'sp'}, dimensions={0}, use_global_device_ids=true | all-gather | bytes 655360 | tf_op jit(solution)/shard_map/all_gather | solution.py:14
  37.5 3.3 while.34
  37.5 0.7 broadcast_select_fusion.6
  38.3 0.7 broadcast_select_fusion.6
  39.2 0.7 broadcast_select_fusion.6
  40.0 0.7 broadcast_select_fusion.6
  41.0 1.1 copy.76
  42.1 0.8 convert_bitcast_fusion
  42.8 1.1 copy.77
  44.1 11.7 %while.33 = (s32[]{:T(128)}, f32[2,128,128]{2,1,0:T(8,128)S(1)}, f32[2]{0:T(128)S(1)}, f32[3,2,128,128]{3,2,0,1:T(8,128)}, f32[3,2,128]{2,1,0:T(2,128)S(1)}, /*i...) while((s32[]{:T(128)}, f32[2,128,128]{2,1,0:T(8,128)S(1)}, ...), condition=%wide.region_9.10_spmd.clone, body=%wide.region_5.9_spmd.clone.sunk | while | flops 201835776 | bytes 1911509 | solution.py:64
  44.6 0.9 fusion.92
  46.5 0.9 fusion.95
  47.5 0.5 convolution_add_fusion.2
  48.5 0.9 fusion.92
  50.4 0.9 fusion.95
  51.4 0.5 convolution_add_fusion.2
  52.4 0.9 fusion.92
  54.2 0.9 fusion.95
  55.3 0.5 convolution_add_fusion.2
  55.8 1.2 fusion.46
  57.0 1.2 fusion.44
  58.7 4.3 convolution_convert_fusion.1
  63.0 0.8 broadcast_multiply_fusion.1
  64.7 39.1 %reduce-scatter.3.cloned.1.call-done = bf16[48,4096]{1,0:T(8,128)(2,1)} async-done(((bf16[384,4096]{1,0:T(8,128)(2,1)}), bf16[48,4096]{1,0:T(8,128)(2,1)}) %reduce-scatter.3.cloned.1.call-update) | async-done | bytes 393232 | tf_op jit(solution)/shard_map/reduce_scatter | solution.py:175
  103.8 1.4 fusion.39
  105.4 2.7 gather_fusion
  108.0 1.6 broadcast_select_fusion.4
  109.6 21.1 %all_to_all.10 = bf16[4,48,4096]{2,1,0:T(8,128)(2,1)} all-to-all(bf16[4,48,4096]{2,1,0:T(8,128)(2,1)S(1)} %broadcast_select_fusion.4), channel_id=1, replica_groups=mesh['sp'=4,'tp'=8] {'sp'}, dimensions={0} | all-to-all | bytes 3145728 | tf_op jit(solution)/shard_map/all_to_all | solution.py:189
  131.0 116.1 %all-gather.5.cloned.1.call-done = bf16[32,48,4096]{2,1,0:T(8,128)(2,1)} async-done(((bf16[4,48,4096]{2,1,0:T(8,128)(2,1)}), bf16[32,48,4096]{2,1,0:T(8,128)(2,1)}) %all-gather.5.cloned.1.call-update) | async-done | bytes 12582928 | tf_op jit(solution)/shard_map/all_gather | solution.py:190
  247.1 9.9 %fusion.33 = f32[32,48,256]{2,1,0:T(8,128)} fusion(bf16[32,48,4096]{2,1,0:T(8,128)(2,1)} %all-gather.5.cloned.1.call-done, bf16[1,4096,256]{2,1,0:T(8,128)(2,1)} %param.33), kind=kOutput, calls=%fused_computation.59 | convolution fusion | flops 3221225472 | bytes 16252928 | tf_op jit(solution)/shard_map/rcd,df->rcf/dot_general | solution.py:191
  257.0 19.4 %convolution_convert_fusion = bf16[32,48,4096]{2,1,0:T(8,128)(2,1)} fusion(bf16[1,256,4096]{2,1,0:T(8,128)(2,1)S(1)} %copy-done, f32[32,48,256]{2,1,0:T(8,128)} %fusion.33, bf16[32,48,4096]{2,1,0:T(8,128)(2,1)} %all-gather.5.cloned.1.call-done, bf16[1,4096,256]{2,1,0:T(8,128)(2,1)} %param.34), kind=kOutput, calls=%fused_computation.54 | convolution fusion | flops 6451101696 | bytes 30932992 | tf_op jit(solution)/shard_map/rcf,fd->rcd/dot_general | solution.py:195
  276.4 127.5 %reduce-scatter.5.cloned.1.call-done = bf16[4,48,4096]{2,1,0:T(8,128)(2,1)} async-done(((bf16[32,48,4096]{2,1,0:T(8,128)(2,1)}), bf16[4,48,4096]{2,1,0:T(8,128)(2,1)}) %reduce-scatter.5.cloned.1.call-update) | async-done | bytes 1572880 | tf_op jit(solution)/shard_map/reduce_scatter | solution.py:194
  403.9 4.6 %all-to-all-start.1 = ((bf16[4,48,4096]{2,1,0:T(8,128)(2,1)}), bf16[4,48,4096]{2,1,0:T(8,128)(2,1)}, u32[]{:S(2)}, u32[]{:S(2)}) async-start(bf16[4,48,4096]{2,1,0:T(8,128)(2,1)} %reduce-scatter.5.cloned.1.call-done), calls=%async_computation.3 | async-start | bytes 3145728 | tf_op jit(solution)/shard_map/all_to_all | solution.py:202
  408.7 0.8 constant_dynamic-slice_fusion.5
  409.6 16.4 %all-to-all-done.1 = bf16[4,48,4096]{2,1,0:T(8,128)(2,1)} async-done(((bf16[4,48,4096]{2,1,0:T(8,128)(2,1)}), bf16[4,48,4096]{2,1,0:T(8,128)(2,1)}, u32[]{:S(2)}, u32[]{:S(2)}) %all-to-all-start.1) | async-done | bytes 1572896 | tf_op jit(solution)/shard_map/all_to_all | solution.py:202
  426.0 3.4 gather_fusion.1
  429.4 2.1 reshape.291
  431.5 3.6 multiply_reduce_fusion
  435.1 0.8 fusion.42
  (97 shorter events, 9.2 us)
Async XLA Ops:
  6.5 250.4 %copy-start = (bf16[1,256,4096]{2,1,0:T(8,128)(2,1)S(1)}, bf16[1,256,4096]{2,1,0:T(8,128)(2,1)}, u32[]{:S(2)}) copy-start(bf16[1,256,4096]{2,1,0:T(8,128)(2,1)} %param.35) | copy-start | bytes 6291460
  6.5 97.3 %reduce-scatter.3.cloned.1.call-start = ((), (), s32[]{:S(2)}) async-start(), calls=%async_computation.4 | async-start | bytes 3538944 | tf_op jit(solution)/shard_map/reduce_scatter | solution.py:175
  44.1 12.9 %copy-start.3 = (f32[256]{0:T(256)S(1)}, f32[256]{0:T(256)}, u32[]{:S(2)}) copy-start(f32[256]{0:T(256)} %param.27) | copy-start | bytes 3076
  55.8 2.6 copy-start.1
  63.0 42.2 %copy-start.2 = (f32[4096]{0:T(1024)S(1)}, f32[4096]{0:T(1024)}, u32[]{:S(2)}) copy-start(f32[4096]{0:T(1024)} %param.30) | copy-start | bytes 49156
  63.0 184.1 %all-gather.5.cloned.1.call-start = ((), (), s32[]{:S(2)}) async-start(), calls=%async_computation.5 | async-start | bytes 14155776 | tf_op jit(solution)/shard_map/all_gather | solution.py:190
  130.8 273.1 %reduce-scatter.5.cloned.1.call-start = ((), (), s32[]{:S(2)}) async-start(), calls=%async_computation.6 | async-start | bytes 14155776 | tf_op jit(solution)/shard_map/reduce_scatter | solution.py:194
  403.9 22.1 %all-to-all-start.1 = ((bf16[4,48,4096]{2,1,0:T(8,128)(2,1)}), bf16[4,48,4096]{2,1,0:T(8,128)(2,1)}, u32[]{:S(2)}, u32[]{:S(2)}) async-start(bf16[4,48,4096]{2,1,0:T(8,128)(2,1)} %reduce-scatter.5.cloned.1.call-done), calls=%async_computation.3 | async-start | bytes 3145728 | tf_op jit(solution)/shard_map/all_to_all | solution.py:202
Sparse Core Ops, SparseCore 0:
  63.1 40.6 reduce-scatter.2
  130.9 116.1 all-gather.4
  276.5 127.3 reduce-scatter.4
where the time goes:
time: 443 us; the launch traced here: 442 us
  waiting for transfers between devices  299 us (67%)
  blocking collectives  42.3 us (10%)
  matrix products  40.3 us (9%)
  other arithmetic  23.5 us (5%)
  local copies, waits for them, and re-layouts  18.1 us (4%)
  between operations  14.1 us (3%)
  starting transfers between devices  4.82 us (1%)
    reduce_scatter x1, waiting for transfers between devices, local(): lax.psum_scatter(jnp.einsum('rcf,fd->rcd', hidden, down_local, preferred_...  127 us
    all_gather x1, waiting for transfers between devices, local(): piece = lax.all_gather(arrived, 'tp', axis=0, tiled=True)  116 us
    reduce_scatter x1, waiting for transfers between devices, local(): lax.psum_scatter(jnp.dot(cell_out, cell_output_matrix, preferred_element_...  39.1 us
    all_to_all x1, blocking collectives, local(): lax.all_to_all(sent, 'sp', split_axis=0, concat_axis=0, tiled=True)  21.1 us
    dot_general x1, matrix products, local(): jnp.einsum('rcf,fd->rcd', hidden, down_local, preferred_element_type=jnp....  19.4 us
    all_to_all x1, waiting for transfers between devices, local(): lax.all_to_all(summed, 'sp', split_axis=0, concat_axis=0, tiled=True)  16.4 us
    unnamed x1, blocking collectives  11.4 us
    dot_general x1, matrix products, local(): jnp.einsum('rcd,df->rcf', piece, gate_local, preferred_element_type=jnp.f...  9.86 us
  transfers between devices with their start and end apart: 4, of which 4 were waited for; matrix products, arithmetic and copies ran while one was open for 1% of the time, Pallas kernels for 0%

commit v1 on v0

--- a/solution.py
+++ b/solution.py
@@ -187,7 +187,12 @@
     moe_in = rms_scale(after_mix, expert_norm_gain)
     sent = fill_slots(moe_in, source).reshape(experts, capacity, moe_in.shape[1])
     arrived = lax.all_to_all(sent, "sp", split_axis=0, concat_axis=0, tiled=True)
-    piece = lax.all_gather(arrived, "tp", axis=0, tiled=True)
+    ring = [arrived]
+    for hop in range(7):
+        ring.append(lax.ppermute(ring[-1], "tp", [(dev, (dev + 1) % 8) for dev in range(8)]))
+    piece = jnp.roll(
+        jnp.concatenate(ring[::-1], axis=0), (lax.axis_index("tp") + 1) * ring[0].shape[0], axis=0
+    )
     gate = jnp.einsum("rcd,df->rcf", piece, gate_local, preferred_element_type=jnp.float32)
     upper = jnp.einsum("rcd,df->rcf", piece, up_local, preferred_element_type=jnp.float32)
     hidden = (jax.nn.silu(gate) * upper).astype(jnp.bfloat16)

time: 443 us -> 513 us (1.16)
  local copies, waits for them, and re-layouts: 18.1 us -> 55.7 us
  waiting for transfers between devices: 299 us -> 333 us
    ppermute x0 -> x7, waiting for transfers between devices: none -> 152 us  [local(): lax.ppermute(ring[-1], 'tp', [(dev, (dev + 1) % 8) for dev in range(8)])]
    all_gather x1 -> x0, waiting for transfers between devices: 116 us -> none  [local(): piece = lax.all_gather(arrived, 'tp', axis=0, tiled=True)]
    unnamed x19 -> x60, local copies, waits for them, and re-layouts: 5.24 us -> 41.6 us
  transfers between devices with their start and end apart: 4 -> 10, of which waited for: 4 -> 10; matrix products, arithmetic and copies ran while one was open for 1% -> 1% of each run, Pallas kernels for 0% -> 0%
where the time goes in v1:
time: 513 us; the launch traced here: 512 us
  waiting for transfers between devices  333 us (65%)
  local copies, waits for them, and re-layouts  55.7 us (11%)
  blocking collectives  42.2 us (8%)
  matrix products  38.1 us (7%)
  other arithmetic  23.5 us (5%)
  between operations  14.4 us (3%)
    ppermute x7, waiting for transfers between devices, local(): lax.ppermute(ring[-1], 'tp', [(dev, (dev + 1) % 8) for dev in range(8)])  152 us
    reduce_scatter x1, waiting for transfers between devices, local(): lax.psum_scatter(jnp.einsum('rcf,fd->rcd', hidden, down_local, preferred_...  126 us
    unnamed x60, local copies, waits for them, and re-layouts  41.6 us
    reduce_scatter x1, waiting for transfers between devices, local(): lax.psum_scatter(jnp.dot(cell_out, cell_output_matrix, preferred_element_...  39.1 us
    all_to_all x1, blocking collectives, local(): lax.all_to_all(sent, 'sp', split_axis=0, concat_axis=0, tiled=True)  21 us
    dot_general x1, matrix products, local(): jnp.einsum('rcf,fd->rcd', hidden, down_local, preferred_element_type=jnp....  19.6 us
    all_to_all x1, waiting for transfers between devices, local(): lax.all_to_all(summed, 'sp', split_axis=0, concat_axis=0, tiled=True)  16.4 us
    unnamed x1, blocking collectives  11.4 us
  transfers between devices with their start and end apart: 10, of which 10 were waited for; matrix products, arithmetic and copies ran while one was open for 1% of the time, Pallas kernels for 0%

profile of v1, /device:TPU:0, one launch (start us, length us, event | category | flops | bytes accessed | tf_op | source)
XLA Modules:
  0.0 512.2 jit_solution(7033482047093833994)
XLA Ops:
  10.3 1.3 dynamic-slice
  12.7 11.4 %all-reduce.2 = (f32[8]{0:T(128)S(1)}, f32[8]{0:T(128)S(1)}) all-reduce(f32[8]{0:T(128)S(1)} %dynamic-update-slice, f32[8]{0:T(128)S(1)} %dynamic-update-slice.1), channel_id=2, replica_groups=mesh['sp'=4,'tp'=8] {'sp'}, use_global_device_ids=true, to_apply=%add | all-reduce | flops 16 | bytes 128
  27.7 9.8 %all-gather.2 = f32[8,128,128]{2,1,0:T(8,128)S(1)} all-gather(f32[2,128,128]{2,1,0:T(8,128)S(1)} %fusion.47), channel_id=4, replica_groups=mesh['sp'=4,'tp'=8] {'sp'}, dimensions={0}, use_global_device_ids=true | all-gather | bytes 655360 | tf_op jit(solution)/shard_map/all_gather | solution.py:14
  37.5 3.3 while.34
  42.8 1.1 copy.77
  44.1 11.7 %while.33 = (s32[]{:T(128)}, f32[2,128,128]{2,1,0:T(8,128)S(1)}, f32[2]{0:T(128)S(1)}, f32[3,2,128,128]{3,2,0,1:T(8,128)}, f32[3,2,128]{2,1,0:T(2,128)S(1)}, /*i...) while((s32[]{:T(128)}, f32[2,128,128]{2,1,0:T(8,128)S(1)}, ...), condition=%wide.region_9.10_spmd.clone, body=%wide.region_5.9_spmd.clone.sunk | while | flops 201835776 | bytes 1911509 | solution.py:64
  55.8 1.2 fusion.44
  57.0 1.2 fusion.42
  58.7 4.3 convolution_convert_fusion.1
  64.7 39.1 %reduce-scatter.3.cloned.1.call-done = bf16[48,4096]{1,0:T(8,128)(2,1)} async-done(((bf16[384,4096]{1,0:T(8,128)(2,1)}), bf16[48,4096]{1,0:T(8,128)(2,1)}) %reduce-scatter.3.cloned.1.call-update) | async-done | bytes 393232 | tf_op jit(solution)/shard_map/reduce_scatter | solution.py:175
  103.8 1.4 fusion.37
  105.4 2.7 gather_fusion
  108.0 1.6 broadcast_select_fusion.4
  109.6 21.0 %all_to_all.10 = bf16[4,48,4096]{2,1,0:T(8,128)(2,1)S(1)} all-to-all(bf16[4,48,4096]{2,1,0:T(8,128)(2,1)S(1)} %broadcast_select_fusion.4), channel_id=1, replica_groups=mesh['sp'=4,'tp'=8] {'sp'}, dimensions={0} | all-to-all | bytes 3145728 | tf_op jit(solution)/shard_map/all_to_all | solution.py:189
  131.8 21.6 %collective-permute-done = bf16[4,48,4096]{2,1,0:T(8,128)(2,1)S(1)} collective-permute-done((bf16[4,48,4096]{2,1,0:T(8,128)(2,1)S(1)}, bf16[4,48,4096]{2,1,0:T(8,128)(2,1)S(1)}, u32[]{:S(2)}, u32[]{:S(2)}) %collective-permute-start) | collective-permute-done | bytes 1572896 | tf_op jit(solution)/shard_map/ppermute | solution.py:192
  153.4 1.2 copy-done.3
  154.6 21.6 %collective-permute-done.1 = bf16[4,48,4096]{2,1,0:T(8,128)(2,1)S(1)} collective-permute-done((bf16[4,48,4096]{2,1,0:T(8,128)(2,1)S(1)}, bf16[4,48,4096]{2,1,0:T(8,128)(2,1)S(1)}, u32[]{:S(2)}, u32[]{:S(2)}) %collective-permute-start.1) | collective-permute-done | bytes 1572896 | tf_op jit(solution)/shard_map/ppermute | solution.py:192
  176.2 1.2 copy-done.5
  177.4 21.6 %collective-permute-done.2 = bf16[4,48,4096]{2,1,0:T(8,128)(2,1)S(1)} collective-permute-done((bf16[4,48,4096]{2,1,0:T(8,128)(2,1)S(1)}, bf16[4,48,4096]{2,1,0:T(8,128)(2,1)S(1)}, u32[]{:S(2)}, u32[]{:S(2)}) %collective-permute-start.2) | collective-permute-done | bytes 1572896 | tf_op jit(solution)/shard_map/ppermute | solution.py:192
  200.2 21.6 %collective-permute-done.3 = bf16[4,48,4096]{2,1,0:T(8,128)(2,1)S(1)} collective-permute-done((bf16[4,48,4096]{2,1,0:T(8,128)(2,1)S(1)}, bf16[4,48,4096]{2,1,0:T(8,128)(2,1)S(1)}, u32[]{:S(2)}, u32[]{:S(2)}) %collective-permute-start.3) | collective-permute-done | bytes 1572896 | tf_op jit(solution)/shard_map/ppermute | solution.py:192
  223.0 21.6 %collective-permute-done.4 = bf16[4,48,4096]{2,1,0:T(8,128)(2,1)S(1)} collective-permute-done((bf16[4,48,4096]{2,1,0:T(8,128)(2,1)S(1)}, bf16[4,48,4096]{2,1,0:T(8,128)(2,1)S(1)}, u32[]{:S(2)}, u32[]{:S(2)}) %collective-permute-start.4) | collective-permute-done | bytes 1572896 | tf_op jit(solution)/shard_map/ppermute | solution.py:192
  244.6 1.2 copy-done.11
  245.8 21.7 %collective-permute-done.5 = bf16[4,48,4096]{2,1,0:T(8,128)(2,1)} collective-permute-done((bf16[4,48,4096]{2,1,0:T(8,128)(2,1)S(1)}, bf16[4,48,4096]{2,1,0:T(8,128)(2,1)}, u32[]{:S(2)}, u32[]{:S(2)}) %collective-permute-start.5) | collective-permute-done | bytes 1572896 | tf_op jit(solution)/shard_map/ppermute | solution.py:192
  267.6 22.0 %collective-permute-done.6 = bf16[4,48,4096]{2,1,0:T(8,128)(2,1)} collective-permute-done((bf16[4,48,4096]{2,1,0:T(8,128)(2,1)}, bf16[4,48,4096]{2,1,0:T(8,128)(2,1)}, u32[]{:S(2)}, u32[]{:S(2)}) %collective-permute-start.6) | collective-permute-done | bytes 1572896 | tf_op jit(solution)/shard_map/ppermute | solution.py:192
  289.5 2.7 constant_dynamic-update-slice_fusion.15
  292.2 2.8 constant_dynamic-update-slice_fusion.14
  295.1 1.2 constant_dynamic-update-slice_fusion.13
  297.0 1.3 constant_dynamic-update-slice_fusion.12
  299.0 1.2 constant_dynamic-update-slice_fusion.11
  301.0 1.3 constant_dynamic-update-slice_fusion.10
  303.0 1.3 constant_dynamic-update-slice_fusion.9
  304.9 1.2 constant_dynamic-update-slice_fusion.8
  306.2 2.8 constant_dynamic-update-slice_fusion.7
  308.9 2.7 constant_dynamic-update-slice_fusion.6
  311.6 1.3 constant_dynamic-update-slice_fusion.5
  312.9 1.3 constant_dynamic-update-slice_fusion.4
  314.2 1.3 constant_dynamic-update-slice_fusion.3
  315.4 1.3 constant_dynamic-update-slice_fusion.2
  316.7 1.3 constant_dynamic-update-slice_fusion.1
  318.0 1.3 constant_dynamic-update-slice_fusion
  320.2 7.6 %fusion.30 = f32[32,48,256]{2,1,0:T(8,128)} fusion(bf16[64,48,4096]{2,1,0:T(8,128)(2,1)} %constant_dynamic-update-slice_fusion, s32[]{:T(128)S(6)} %select_n.112, bf16[1,4096,256]{2,1,0:T(8,128)(2,1)S(1)} %copy-done.16), kind=kOutput, calls=%fused_computation.54 | convolution fusion | flops 3221225472 | bytes 16252932 | tf_op jit(solution)/shard_map/rcd,df->rcf/dot_general | solution.py:197
  327.8 19.6 %convolution_convert_fusion = bf16[32,48,4096]{2,1,0:T(8,128)(2,1)} fusion(bf16[1,256,4096]{2,1,0:T(8,128)(2,1)S(1)} %copy-done, f32[32,48,256]{2,1,0:T(8,128)} %fusion.30, bf16[64,48,4096]{2,1,0:T(8,128)(2,1)} %constant_dynamic-update-slice_fusion, s32[]{:T(128)S(6)} %select_n.112, bf16[1,4096,256]{2,1,0:T(8,128)(2,1)} %param.33), kind=kOutput, calls=%fused_computation.58 | convolution fusion | flops 6451101696 | bytes 30932996 | tf_op jit(solution)/shard_map/rcf,fd->rcd/dot_general | solution.py:200
  347.4 126.0 %reduce-scatter.5.cloned.1.call-done = bf16[4,48,4096]{2,1,0:T(8,128)(2,1)} async-done(((bf16[32,48,4096]{2,1,0:T(8,128)(2,1)}), bf16[4,48,4096]{2,1,0:T(8,128)(2,1)}) %reduce-scatter.5.cloned.1.call-update) | async-done | bytes 1572880 | tf_op jit(solution)/shard_map/reduce_scatter | solution.py:199
  473.3 4.6 all-to-all-start.1
  479.0 16.4 %all-to-all-done.1 = bf16[4,48,4096]{2,1,0:T(8,128)(2,1)} async-done(((bf16[4,48,4096]{2,1,0:T(8,128)(2,1)}), bf16[4,48,4096]{2,1,0:T(8,128)(2,1)}, u32[]{:S(2)}, u32[]{:S(2)}) %all-to-all-start.1) | async-done | bytes 1572896 | tf_op jit(solution)/shard_map/all_to_all | solution.py:207
  495.4 3.4 gather_fusion.1
  498.8 2.1 reshape.291
  500.9 3.6 multiply_reduce_fusion
  (150 shorter events, 36.6 us)
Async XLA Ops:
  6.5 321.2 %copy-start = (bf16[1,256,4096]{2,1,0:T(8,128)(2,1)S(1)}, bf16[1,256,4096]{2,1,0:T(8,128)(2,1)}, u32[]{:S(2)}) copy-start(bf16[1,256,4096]{2,1,0:T(8,128)(2,1)} %param.35) | copy-start | bytes 6291460
  6.5 97.3 %reduce-scatter.3.cloned.1.call-start = ((), (), s32[]{:S(2)}) async-start(), calls=%async_computation.4 | async-start | bytes 3538944 | tf_op jit(solution)/shard_map/reduce_scatter | solution.py:175
  44.1 12.9 %copy-start.15 = (f32[256]{0:T(256)S(1)}, f32[256]{0:T(256)}, u32[]{:S(2)}) copy-start(f32[256]{0:T(256)} %param.27) | copy-start | bytes 3076
  55.8 2.6 copy-start.13
  63.0 42.2 %copy-start.14 = (f32[4096]{0:T(1024)S(1)}, f32[4096]{0:T(1024)}, u32[]{:S(2)}) copy-start(f32[4096]{0:T(1024)} %param.30) | copy-start | bytes 49156
  63.0 410.3 %reduce-scatter.5.cloned.1.call-start = ((), (), s32[]{:S(2)}) async-start(), calls=%async_computation.5 | async-start | bytes 14155776 | tf_op jit(solution)/shard_map/reduce_scatter | solution.py:199
  130.7 1.1 copy-start.1
  131.8 21.6 %collective-permute-start = (bf16[4,48,4096]{2,1,0:T(8,128)(2,1)S(1)}, bf16[4,48,4096]{2,1,0:T(8,128)(2,1)S(1)}, u32[]{:S(2)}, u32[]{:S(2)}) collective-permute-start(bf16[4,48,4096]{2,1,0:T(8,128)(2,1)S(1)} %all_to_all.10), channel_id=1, source_target_pairs={{0,1},{1,2},{2,3},{3,4},{4,5},{5,6},{6,7},{7,0},{8,9},{9,10},{10,1... | collective-permute-start | bytes 4718600 | tf_op jit(solution)/shard_map/ppermute | solution.py:192
  153.4 1.2 copy-start.3
  154.6 21.6 %collective-permute-start.1 = (bf16[4,48,4096]{2,1,0:T(8,128)(2,1)S(1)}, bf16[4,48,4096]{2,1,0:T(8,128)(2,1)S(1)}, u32[]{:S(2)}, u32[]{:S(2)}) collective-permute-start(bf16[4,48,4096]{2,1,0:T(8,128)(2,1)S(1)} %collective-permute-done), channel_id=1, source_target_pairs={{0,1},{1,2},{2,3},{3,4},{4,5},{5,6},{6,7},{7,0},{8,9},{9,10},{10,1... | collective-permute-start | bytes 4718600 | tf_op jit(solution)/shard_map/ppermute | solution.py:192
  176.2 1.2 copy-start.5
  177.4 21.6 %collective-permute-start.2 = (bf16[4,48,4096]{2,1,0:T(8,128)(2,1)S(1)}, bf16[4,48,4096]{2,1,0:T(8,128)(2,1)S(1)}, u32[]{:S(2)}, u32[]{:S(2)}) collective-permute-start(bf16[4,48,4096]{2,1,0:T(8,128)(2,1)S(1)} %collective-permute-done.1), channel_id=1, source_target_pairs={{0,1},{1,2},{2,3},{3,4},{4,5},{5,6},{6,7},{7,0},{8,9},{9,10},{10,1... | collective-permute-start | bytes 4718600 | tf_op jit(solution)/shard_map/ppermute | solution.py:192
  199.1 1.1 copy-start.7
  200.2 21.6 %collective-permute-start.3 = (bf16[4,48,4096]{2,1,0:T(8,128)(2,1)S(1)}, bf16[4,48,4096]{2,1,0:T(8,128)(2,1)S(1)}, u32[]{:S(2)}, u32[]{:S(2)}) collective-permute-start(bf16[4,48,4096]{2,1,0:T(8,128)(2,1)S(1)} %collective-permute-done.2), channel_id=1, source_target_pairs={{0,1},{1,2},{2,3},{3,4},{4,5},{5,6},{6,7},{7,0},{8,9},{9,10},{10,1... | collective-permute-start | bytes 4718600 | tf_op jit(solution)/shard_map/ppermute | solution.py:192
  221.8 1.1 copy-start.9
  223.0 21.6 %collective-permute-start.4 = (bf16[4,48,4096]{2,1,0:T(8,128)(2,1)S(1)}, bf16[4,48,4096]{2,1,0:T(8,128)(2,1)S(1)}, u32[]{:S(2)}, u32[]{:S(2)}) collective-permute-start(bf16[4,48,4096]{2,1,0:T(8,128)(2,1)S(1)} %collective-permute-done.3), channel_id=1, source_target_pairs={{0,1},{1,2},{2,3},{3,4},{4,5},{5,6},{6,7},{7,0},{8,9},{9,10},{10,1... | collective-permute-start | bytes 4718600 | tf_op jit(solution)/shard_map/ppermute | solution.py:192
  244.6 1.2 copy-start.11
  245.8 21.7 %collective-permute-start.5 = (bf16[4,48,4096]{2,1,0:T(8,128)(2,1)S(1)}, bf16[4,48,4096]{2,1,0:T(8,128)(2,1)}, u32[]{:S(2)}, u32[]{:S(2)}) collective-permute-start(bf16[4,48,4096]{2,1,0:T(8,128)(2,1)S(1)} %collective-permute-done.4), channel_id=1, source_target_pairs={{0,1},{1,2},{2,3},{3,4},{4,5},{5,6},{6,7},{7,0},{8,9},{9,10},{10,1... | collective-permute-start | bytes 4718600 | tf_op jit(solution)/shard_map/ppermute | solution.py:192
  267.6 22.0 %collective-permute-start.6 = (bf16[4,48,4096]{2,1,0:T(8,128)(2,1)}, bf16[4,48,4096]{2,1,0:T(8,128)(2,1)}, u32[]{:S(2)}, u32[]{:S(2)}) collective-permute-start(bf16[4,48,4096]{2,1,0:T(8,128)(2,1)} %collective-permute-done.5), channel_id=1, source_target_pairs={{0,1},{1,2},{2,3},{3,4},{4,5},{5,6},{6,7},{7,0},{8,9},{9,10},{10,1... | collective-permute-start | bytes 4718600 | tf_op jit(solution)/shard_map/ppermute | solution.py:192
  292.2 2.8 copy-start.12
  295.1 2.0 copy-start.10
  297.0 2.0 copy-start.8
  299.0 2.0 copy-start.6
  301.0 2.0 copy-start.4
  303.0 2.0 copy-start.2
  318.0 2.2 copy-start.16
  473.3 22.1 %all-to-all-start.1 = ((bf16[4,48,4096]{2,1,0:T(8,128)(2,1)}), bf16[4,48,4096]{2,1,0:T(8,128)(2,1)}, u32[]{:S(2)}, u32[]{:S(2)}) async-start(bf16[4,48,4096]{2,1,0:T(8,128)(2,1)} %reduce-scatter.5.cloned.1.call-done), calls=%async_computation.3 | async-start | bytes 3145728 | tf_op jit(solution)/shard_map/all_to_all | solution.py:207
Sparse Core Ops, SparseCore 0:
  63.1 40.6 reduce-scatter.2
  347.5 125.8 reduce-scatter.4
